TPU v7x, 512 devices: a whole 4x4x16 slice. The times are simulated.
512 devices in a mesh: sp: 64 (over z, y), tp: 8 (over x, core).
Axes of the slice: x: 4, y: 4, z: 16, core: 2. Of those that a mesh axis runs over, the one named last changes fastest.
Arguments:
- residual_signal: bfloat16 [16384, 2048], P('sp'), may hold values from -6 to 6
- reading_probe_preactivations: bfloat16 [16384, 1024], P('sp', 'tp'), may hold values from -6 to 6
- keep_switch_preactivations: bfloat16 [16384, 1024], P('sp', 'tp'), may hold values from -5.5 to 5.5
- written_entries: bfloat16 [16384, 1024], P('sp', 'tp'), may hold values from -6 to 6
- emission_switch_preactivations: bfloat16 [16384, 1024], P('sp', 'tp'), may hold values from -6 to 6
- additional_shrink_amount: float32 [16384, 1024], P('sp', 'tp'), may hold values from -0.7 to 0
- complement_of_floor: float32 [1024], P('tp'), may hold values from 6.1035156e-06 to 0.1
- per_group_rescaler: float32 [128], replicated, may hold values from 0.1 to 1.9
- emission_linear_map: bfloat16 [1024, 2048], P('tp'), may hold values from -0.1875 to 0.1875
- channel_layer_rescaler: float32 [2048], replicated, may hold values from 0.1 to 1.9
- expanding_linear_map: bfloat16 [2048, 8192], P('sp', 'tp'), may hold values from -0.125 to 0.125
- contracting_linear_map: bfloat16 [2048, 8192], P('sp', 'tp'), may hold values from -0.0625 to 0.0625
Outputs:
- layer_out: bfloat16 [16384, 2048], P('sp')
All inputs are finite; a program needn't handle non-finite values.
Results may differ from a plain program's by a relative error of at most 0.006.
Values may be sent and summed in bfloat16 or wider, within the bound.
A program may use at most 64 MiB of HBM per device.

v0:
```python
import jax
import jax.numpy as jnp
from jax import lax
from jax.sharding import Mesh
from jax.sharding import PartitionSpec as P

HEAD = 128
BLOCK = 64
SP = ("sp_0", "sp_1")
norm_eps = 1e-06
HIGH_ACCURACY = lax.Precision.HIGHEST


def filled_with(shard, identity):
    return jax.tree.map(
        lambda a, e: jnp.broadcast_to(jnp.asarray(e, a.dtype), a.shape), shard, identity
    )


def gathered_once(shard, axis):
    leaves = jax.tree.leaves(shard)
    turns = sorted(range(len(leaves)), key=lambda k: -leaves[k].size)
    width = (1, *leaves[turns[0]].shape)[-1]
    lines = [
        jnp.pad(leaves[k].reshape(-1), (0, -leaves[k].size % width)).reshape(-1, width)
        for k in turns
    ]
    both, at, found = (lax.all_gather(jnp.concatenate(lines), axis), 0, {})
    for k, line in zip(turns, lines):
        piece = both[:, at : at + len(line)].reshape(len(both), -1)
        found[k] = piece[:, : leaves[k].size].reshape(-1, *leaves[k].shape)
        at += len(line)
    numbers = iter(range(len(leaves)))
    return jax.tree.map(lambda _: found[next(numbers)], shard)


def entering(shard, axes, combine, identity):
    before = start = filled_with(shard, identity)
    total = shard
    for axis in reversed(axes):
        peers, index = (lax.axis_size(axis), lax.axis_index(axis))
        pieces = gathered_once(total, axis)
        inside, total = (start, start)
        for k in range(peers):
            passed = k < index
            total = combine(total, jax.tree.map(lambda part: part[k], pieces))
            inside = jax.tree.map(lambda new, old: jnp.where(passed, new, old), total, inside)
        before = combine(inside, before)
    return before


def laid_out(blocks, dim):
    lengths = list(blocks.shape[1:])
    lengths[dim] *= blocks.shape[0]
    return jnp.moveaxis(blocks, 0, dim).reshape(lengths)


def copy_for_each(shard, axis):
    peers = lax.axis_size(axis)
    return lax.all_to_all(
        jnp.broadcast_to(shard[None], (peers, *shard.shape)), axis, 0, 0, tiled=True
    )


def gathered_copies(shard, axis, dim):
    return laid_out(copy_for_each(shard, axis), dim)


def in_one_piece(arrays, axis, dim, along):
    widths = [a.shape[along] for a in arrays]
    both = jnp.concatenate(arrays, axis=along)
    whole = lax.all_gather(both, axis, axis=dim, tiled=True)
    return tuple(jnp.split(whole, [sum(widths[:k]) for k in range(1, len(widths))], axis=along))


def cut_along(shard, dim, peers):
    lengths = shard.shape
    blocks = shard.reshape(*lengths[:dim], peers, lengths[dim] // peers, *lengths[dim + 1 :])
    return jnp.moveaxis(blocks, dim, 0)


def sum_at_owner(shard, axis, dim):
    blocks = cut_along(shard, dim, lax.axis_size(axis))
    arrived = lax.all_to_all(blocks, axis, split_axis=0, concat_axis=0, tiled=True)
    return arrived.astype(jnp.float32).sum(axis=0)


def block_step(state_matrix, inputs):
    query_block_rows, key_blk, logs_blk, value_block_rows = inputs
    cumulative_decay = jnp.cumsum(logs_blk, axis=1)
    carried_state = jnp.einsum(
        "rlb,rbz->rlz",
        query_block_rows * jnp.exp(cumulative_decay),
        state_matrix,
        precision=HIGH_ACCURACY,
    )
    spread = cumulative_decay[:, :, None, :] - cumulative_decay[:, None, :, :]
    places = jnp.arange(BLOCK)
    lower = places[:, None] >= places[None, :]
    decay = jnp.exp(jnp.where(lower[None, :, :, None], spread, -jnp.inf))
    scores = jnp.einsum(
        "htk,hsk,htsk->hts", query_block_rows, key_blk, decay, precision=HIGH_ACCURACY
    )
    result = carried_state + jnp.einsum(
        "hts,hsv->htv", scores, value_block_rows, precision=HIGH_ACCURACY
    )
    final_state = cumulative_decay[:, -1:, :]
    decayed_key_rows = key_blk * jnp.exp(final_state - cumulative_decay)
    state_matrix = jnp.exp(final_state[:, 0, :])[..., None] * state_matrix + jnp.einsum(
        "aux,auf->axf", decayed_key_rows, value_block_rows, precision=HIGH_ACCURACY
    )
    return (state_matrix, result)


def combine_carry(earlier, later):
    return (earlier[0] * later[0], later[0][..., None] * earlier[1] + later[1])


def body(
    residual_signal,
    reading_probe_preactivations,
    keep_switch_preactivations,
    written_entries,
    emission_switch_preactivations,
    additional_shrink_amount,
    complement_of_floor,
    per_group_rescaler,
    emission_linear_map,
    channel_layer_rescaler,
    expanding_linear_map,
    contracting_linear_map,
):
    positions = reading_probe_preactivations.shape[0]
    channels = reading_probe_preactivations.shape[1]
    local_heads = channels // HEAD
    count = positions // BLOCK
    query_act = jax.nn.silu(reading_probe_preactivations.astype(jnp.float32))
    logarithmic_keep_fraction = (
        jnp.logaddexp(
            jnp.log1p(-complement_of_floor),
            jnp.log(complement_of_floor)
            + jax.nn.log_sigmoid(keep_switch_preactivations.astype(jnp.float32)),
        )
        + additional_shrink_amount
    )
    key_part = -jnp.expm1(logarithmic_keep_fraction)
    value_part = written_entries.astype(jnp.float32)

    def to_blocks(values):
        return values.reshape(count, BLOCK, local_heads, HEAD).transpose(0, 2, 1, 3)

    start = jnp.zeros((local_heads, HEAD, HEAD), jnp.float32)
    state_end, outputs = lax.scan(
        block_step,
        start,
        (
            to_blocks(query_act),
            to_blocks(key_part),
            to_blocks(logarithmic_keep_fraction),
            to_blocks(value_part),
        ),
    )
    within_block_output = outputs.transpose(0, 2, 1, 3).reshape(positions, local_heads, HEAD)
    running = jnp.cumsum(logarithmic_keep_fraction, axis=0)
    decay_total = jnp.exp(running[-1]).reshape(local_heads, HEAD)
    identity = (
        jnp.ones((local_heads, HEAD), jnp.float32),
        jnp.zeros((local_heads, HEAD, HEAD), jnp.float32),
    )
    prior_state = entering((decay_total, state_end), SP, combine_carry, identity)
    weighted_scores = (query_act * jnp.exp(running)).reshape(positions, local_heads, HEAD)
    recurrent_output = within_block_output + jnp.einsum(
        "pnm,nmx->pnx", weighted_scores, prior_state[1], precision=HIGH_ACCURACY
    )
    scaled = (
        recurrent_output
        * lax.rsqrt(
            jnp.mean(recurrent_output * recurrent_output, axis=-1, keepdims=True) + norm_eps
        )
        * per_group_rescaler
    )
    gated = scaled * jax.nn.silu(emission_switch_preactivations.astype(jnp.float32)).reshape(
        positions, local_heads, HEAD
    )
    mixed_heads = gated.reshape(positions, channels).astype(jnp.bfloat16)
    all_heads = gathered_copies(mixed_heads, "tp", 1)
    full_out = lax.all_gather(emission_linear_map, "tp", axis=0, tiled=True)
    projected = jnp.dot(all_heads, full_out, preferred_element_type=jnp.float32)
    after_mix = residual_signal.astype(jnp.float32) + projected
    normed = (
        after_mix
        * lax.rsqrt(jnp.mean(after_mix * after_mix, axis=-1, keepdims=True) + norm_eps)
        * channel_layer_rescaler
    ).astype(jnp.bfloat16)
    up_whole, down_whole = in_one_piece((expanding_linear_map, contracting_linear_map), SP, 0, 1)
    upward = jnp.dot(normed, up_whole, preferred_element_type=jnp.float32)
    hidden = jnp.square(jax.nn.relu(upward)).astype(jnp.bfloat16)
    share = positions // lax.axis_size("tp")
    downward = sum_at_owner(
        lax.dot_general(
            hidden, down_whole, (((1,), (1,)), ((), ())), preferred_element_type=jnp.float32
        ).astype(jnp.bfloat16),
        "tp",
        0,
    )
    own_start = lax.axis_index("tp") * share
    own_mix = lax.dynamic_slice_in_dim(after_mix, own_start, share, 0)
    finished = (own_mix + downward).astype(jnp.bfloat16)
    return gathered_copies(finished, "tp", 0)


def solution(mesh):
    finer = Mesh(mesh.devices.reshape(16, 4, mesh.shape["tp"]), ("sp_0", "sp_1", "tp"))
    return jax.shard_map(
        body,
        mesh=finer,
        in_specs=(
            P(SP, None),
            P(SP, "tp"),
            P(SP, "tp"),
            P(SP, "tp"),
            P(SP, "tp"),
            P(SP, "tp"),
            P("tp"),
            P(),
            P("tp", None),
            P(),
            P(SP, "tp"),
            P(SP, "tp"),
        ),
        out_specs=P(SP, None),
        check_vma=False,
    )
```

profile of v0, /device:TPU:1, one launch (start us, length us, event | category | flops | bytes accessed | tf_op | source)
XLA Modules:
  0.0 363.2 jit_solution(13176499211492240413)
XLA Ops:
  6.5 0.0 all-gather.12.cloned.1.call-start
  6.5 0.7 negate_log-plus-one_fusion
  7.2 1.1 exponential-minus-one_negate_fusion
  8.4 0.1 fusion.63
  8.6 0.1 copy.45
  8.7 0.1 slice.242
  8.8 0.1 copy.46
  8.9 1.0 copy.41
  9.9 0.1 copy.42
  10.0 0.0 copy-start.2
  10.1 0.0 copy-start.3
  10.1 13.1 %while.13 = (s32[]{:T(128)}, f32[1,128,128]{2,1,0:T(8,128)S(1)}, f32[4,1,64,128]{3,2,1,0:T(8,128)S(1)}, f32[4,1,64,128]{3,2,1,0:T(8,128)S(1)}, f32[4,1,64,128]{3...) while((s32[]{:T(128)}, f32[1,128,128]{2,1,0:T(8,128)S(1)}, ...), condition=%wide.region_2.3_spmd.clone, body=%wide.region_0.2_spmd.clone.sunk | while | flops 34693120 | bytes 5108864 | solution.py:153
  10.1 0.1 reduce_window_sum.34
  10.2 0.6 select_exponential_fusion.2
  10.8 1.7 fusion.174
  12.6 0.2 fusion.173
  12.7 0.2 fusion.175
  13.0 0.3 fusion.172
  13.4 0.1 reduce_window_sum.34
  13.5 0.6 select_exponential_fusion.2
  14.1 1.7 fusion.174
  15.8 0.2 fusion.173
  16.0 0.2 fusion.175
  16.3 0.3 fusion.172
  16.6 0.1 reduce_window_sum.34
  16.7 0.6 select_exponential_fusion.2
  17.4 1.7 fusion.174
  19.1 0.2 fusion.173
  19.3 0.2 fusion.175
  19.5 0.3 fusion.172
  19.9 0.1 reduce_window_sum.34
  20.0 0.6 select_exponential_fusion.2
  20.6 1.7 fusion.174
  22.4 0.2 fusion.173
  22.5 0.2 fusion.175
  22.8 0.3 fusion.172
  23.1 0.0 copy-start.1
  23.2 10.7 %all-gather.2 = f32[4,129,128]{2,1,0:T(8,128)S(1)} all-gather(f32[1,129,128]{2,1,0:T(8,128)S(1)} %maximum_bitcast_fusion), channel_id=2, replica_groups=mesh['sp_0'=16,'sp_1'=4,'tp'=8] {'sp_1'}, dimensions={0}, use_global_device_ids=true | all-gather | bytes 330240 | tf_op jit(solution)/shard_map/all_gather | solution.py:28
  33.9 0.1 fusion.153
  34.1 0.6 maximum_bitcast_fusion.1
  34.7 0.0 all-gather.12.cloned.1.call-update
  34.7 0.0 copy-start.4
  34.7 0.0 all-gather.8.cloned.1.call-start
  34.8 0.7 all-gather.8.cloned.1.call-update
  35.5 0.0 all-gather.10.cloned.1.call-start
  35.6 0.7 pad_maximum_fusion
  36.2 0.0 all-gather.10.cloned.1.call-update
  36.3 0.1 copy.47
  36.4 0.1 copy.48
  36.5 65.5 %all-gather.12.cloned.1.call-done = f32[16,129,128]{2,1,0:T(8,128)} async-done(((f32[1,129,128]{2,1,0:T(8,128)}), f32[16,129,128]{2,1,0:T(8,128)}) %all-gather.12.cloned.1.call-update) | async-done | bytes 1056784 | tf_op jit(solution)/shard_map/all_gather | solution.py:28
  102.1 0.8 slice_bitcast_fusion.16
  102.8 2.1 multiply_reduce_fusion.1
  105.0 0.1 fusion.67
  105.1 24.3 %all_to_all.15 = bf16[8,256,128]{1,2,0:T(8,128)(2,1)S(1)} all-to-all(bf16[8,256,128]{1,2,0:T(8,128)(2,1)S(1)} %broadcast_in_dim.32), channel_id=1, replica_groups=mesh['sp_0'=16,'sp_1'=4,'tp'=8] {'tp'}, dimensions={0} | all-to-all | bytes 1048576 | tf_op jit(solution)/shard_map/all_to_all | solution.py:60
  129.4 22.2 %all-gather.8.cloned.1.call-done = bf16[1024,2048]{1,0:T(8,128)(2,1)} async-done(((bf16[128,2048]{1,0:T(8,128)(2,1)}), bf16[1024,2048]{1,0:T(8,128)(2,1)}) %all-gather.8.cloned.1.call-update) | async-done | bytes 4194320 | tf_op jit(solution)/shard_map/all_gather | solution.py:187
  151.7 3.9 %multiply_reduce_fusion = (f32[256]{0:T(256)S(1)}, f32[256,2048]{1,0:T(8,128)S(1)}) fusion(bf16[256,1024]{0,1:T(8,128)(2,1)S(1)} %bitcast.218, bf16[1024,2048]{1,0:T(8,128)(2,1)} %all-gather.8.cloned.1.call-done, bf16[256,2048]{1,0:T(8,128)(2,1)} %param.14), kind=kOutput, calls=%fused_computation.45 | convolution fusion | flops 1075838720 | bytes 7865344 | tf_op jit(solution)/shard_map/dot_general | solution.py:188
  155.5 147.1 %all-gather.10.cloned.1.call-done = bf16[2048,2048]{1,0:T(8,128)(2,1)} async-done(((bf16[32,2048]{1,0:T(8,128)(2,1)}), bf16[2048,2048]{1,0:T(8,128)(2,1)}) %all-gather.10.cloned.1.call-update) | async-done | bytes 8388624 | tf_op jit(solution)/shard_map/all_gather | solution.py:72
  302.7 6.8 %fusion.32 = bf16[256,2048]{1,0:T(8,128)(2,1)} fusion(bf16[2048,2048]{1,0:T(8,128)(2,1)} %all-gather.10.cloned.1.call-done, f32[256,2048]{1,0:T(8,128)S(1)} %get-tuple-element.142, f32[2048]{0:T(1024)S(1)} %copy-done.5, f32[256]{0:T(256)S(1)} %add_rsqrt_fusion), kind=kOutput, calls=%fused_computation.42 | convolution fusion | flops 2150367232 | bytes 11543552 | tf_op jit(solution)/shard_map/dot_general | solution.py:200
  309.5 12.7 %all-to-all-start.1 = ((bf16[8,32,2048]{2,1,0:T(8,128)(2,1)}), bf16[8,32,2048]{2,1,0:T(8,128)(2,1)S(1)}, u32[]{:S(2)}, u32[]{:S(2)}) async-start(bf16[8,32,2048]{2,1,0:T(8,128)(2,1)} %bitcast.223), calls=%async_computation.1 | async-start | bytes 2097152 | tf_op jit(solution)/shard_map/all_to_all | solution.py:84
  322.2 15.0 %all-to-all-done.1 = bf16[8,32,2048]{2,1,0:T(8,128)(2,1)S(1)} async-done(((bf16[8,32,2048]{2,1,0:T(8,128)(2,1)}), bf16[8,32,2048]{2,1,0:T(8,128)(2,1)S(1)}, u32[]{:S(2)}, u32[]{:S(2)}) %all-to-all-start.1) | async-done | bytes 1048608 | tf_op jit(solution)/shard_map/all_to_all | solution.py:84
  337.1 0.1 convert_reduce_fusion
  337.3 0.1 broadcast_in_dim.33
  337.4 18.3 %all_to_all.16 = bf16[8,32,2048]{2,1,0:T(8,128)(2,1)S(1)} all-to-all(bf16[8,32,2048]{2,1,0:T(8,128)(2,1)S(1)} %broadcast_in_dim.33), channel_id=1, replica_groups=mesh['sp_0'=16,'sp_1'=4,'tp'=8] {'tp'}, dimensions={0} | all-to-all | bytes 2097152 | tf_op jit(solution)/shard_map/all_to_all | solution.py:60
  355.7 1.0 copy.80
  (46 shorter events, 0.4 us)
Async XLA Ops:
  6.5 3.5 copy-start
  6.5 95.5 %all-gather.12.cloned.1.call-start = ((), (), s32[]{:S(2)}) async-start(), calls=%async_computation.5 | async-start | bytes 1183744 | tf_op jit(solution)/shard_map/all_gather | solution.py:28
  10.0 25.5 %copy-start.2 = (bf16[32,1024]{1,0:T(8,128)(2,1)S(1)}, bf16[32,1024]{1,0:T(8,128)(2,1)}, u32[]{:S(2)}) copy-start(bf16[32,1024]{1,0:T(8,128)(2,1)} %param.25) | copy-start | bytes 196612
  10.1 25.5 %copy-start.3 = (bf16[32,1024]{1,0:T(8,128)(2,1)S(1)}, bf16[32,1024]{1,0:T(8,128)(2,1)}, u32[]{:S(2)}) copy-start(bf16[32,1024]{1,0:T(8,128)(2,1)} %param.24) | copy-start | bytes 196612
  23.1 13.3 %copy-start.1 = (bf16[256,128]{1,0:T(8,128)(2,1)S(1)}, bf16[256,128]{1,0:T(8,128)(2,1)}, u32[]{:S(2)}) copy-start(bf16[256,128]{1,0:T(8,128)(2,1)} %param.18) | copy-start | bytes 196612
  34.7 70.2 %copy-start.4 = (f32[128]{0:T(128)S(1)}, f32[128]{0:T(128)}, u32[]{:S(2)}) copy-start(f32[128]{0:T(128)} %param.21) | copy-start | bytes 1540
  34.7 116.9 %all-gather.8.cloned.1.call-start = ((), (), s32[]{:S(2)}) async-start(), calls=%async_computation.3 | async-start | bytes 4718592 | tf_op jit(solution)/shard_map/all_gather | solution.py:187
  35.5 267.2 %all-gather.10.cloned.1.call-start = ((), (), s32[]{:S(2)}) async-start(), calls=%async_computation.4 | async-start | bytes 8519680 | tf_op jit(solution)/shard_map/all_gather | solution.py:72
  151.7 151.0 %copy-start.5 = (f32[2048]{0:T(1024)S(1)}, f32[2048]{0:T(1024)}, u32[]{:S(2)}) copy-start(f32[2048]{0:T(1024)} %param.23) | copy-start | bytes 24580
  309.5 27.6 %all-to-all-start.1 = ((bf16[8,32,2048]{2,1,0:T(8,128)(2,1)}), bf16[8,32,2048]{2,1,0:T(8,128)(2,1)S(1)}, u32[]{:S(2)}, u32[]{:S(2)}) async-start(bf16[8,32,2048]{2,1,0:T(8,128)(2,1)} %bitcast.223), calls=%async_computation.1 | async-start | bytes 2097152 | tf_op jit(solution)/shard_map/all_to_all | solution.py:84
Sparse Core Ops, SparseCore 0:
  34.8 67.1 all-gather.11
  104.2 47.3 all-gather.7
  154.6 148.0 all-gather.9
where the time goes:
time: 364 us; the launch traced here: 363 us
  waiting for transfers between devices  251 us (69%)
  blocking collectives  53.4 us (15%)
  matrix products  15.7 us (4%)
  other arithmetic  14.3 us (4%)
  between operations  13.4 us (4%)
  starting transfers between devices  12.8 us (4%)
    all_gather x1, waiting for transfers between devices, in_one_piece(): whole = lax.all_gather(both, axis, axis=dim, tiled=True)  147 us
    all_gather x1, waiting for transfers between devices, gathered_once(): both, at, found = (lax.all_gather(jnp.concatenate(lines), axis), 0, {})  65.5 us
    all_to_all x2, blocking collectives, copy_for_each(): lax.all_to_all(jnp.broadcast_to(shard[None], (peers, *shard.shape)), axis...  42.6 us
    all_gather x1, waiting for transfers between devices, body(): full_out = lax.all_gather(emission_linear_map, 'tp', axis=0, tiled=True)  22.2 us
    all_to_all x1, waiting for transfers between devices, sum_at_owner(): lax.all_to_all(blocks, axis, split_axis=0, concat_axis=0, tiled=True)  15 us
    all_to_all x1, starting transfers between devices, sum_at_owner(): lax.all_to_all(blocks, axis, split_axis=0, concat_axis=0, tiled=True)  12.7 us
    all_gather x1, blocking collectives, gathered_once(): both, at, found = (lax.all_gather(jnp.concatenate(lines), axis), 0, {})  10.7 us
  transfers between devices with their start and end apart: 4, of which 4 were waited for; matrix products, arithmetic and copies ran while one was open for 2% of the time, Pallas kernels for 0%

commit v1 on v0

--- a/solution.py
+++ b/solution.py
@@ -184,7 +184,12 @@
     )
     mixed_heads = gated.reshape(positions, channels).astype(jnp.bfloat16)
     all_heads = gathered_copies(mixed_heads, "tp", 1)
-    full_out = lax.all_gather(emission_linear_map, "tp", axis=0, tiled=True)
+    ring = [emission_linear_map]
+    for hop in range(7):
+        ring.append(lax.ppermute(ring[-1], "tp", [(dev, (dev + 1) % 8) for dev in range(8)]))
+    full_out = jnp.roll(
+        jnp.concatenate(ring[::-1], axis=0), (lax.axis_index("tp") + 1) * ring[0].shape[0], axis=0
+    )
     projected = jnp.dot(all_heads, full_out, preferred_element_type=jnp.float32)
     after_mix = residual_signal.astype(jnp.float32) + projected
     normed = (

time: 364 us -> 327 us (0.90)
  waiting for transfers between devices: 251 us -> 184 us
  starting transfers between devices: 12.8 us -> 38.9 us
  blocking collectives: 53.4 us -> 29.1 us
  local copies, waits for them, and re-layouts: 2.83 us -> 24.5 us
    all_gather x1, waiting for transfers between devices: 65.5 us -> 14.9 us  [gathered_once(): both, at, found = (lax.all_gather(jnp.concatenate(lines), axis), 0, {})]
    ppermute x0 -> x7, waiting for transfers between devices: none -> 38.6 us  [body(): lax.ppermute(ring[-1], 'tp', [(dev, (dev + 1) % 8) for dev in range(8)])]
    all_gather x1, waiting for transfers between devices: 147 us -> 116 us  [in_one_piece(): whole = lax.all_gather(both, axis, axis=dim, tiled=True)]
    all_to_all x2 -> x1, blocking collectives: 42.6 us -> 18.3 us  [copy_for_each(): lax.all_to_all(jnp.broadcast_to(shard[None], (peers, *shard.shape)), axis...]
    all_gather x1 -> x0, waiting for transfers between devices: 22.2 us -> none  [body(): full_out = lax.all_gather(emission_linear_map, 'tp', axis=0, tiled=True)]
    ppermute x0 -> x7, starting transfers between devices: none -> 22.1 us  [body(): lax.ppermute(ring[-1], 'tp', [(dev, (dev + 1) % 8) for dev in range(8)])]
    unnamed x17 -> x40, local copies, waits for them, and re-layouts: 2.1 us -> 20.6 us
    all_to_all x0 -> x1, starting transfers between devices: none -> 4.11 us  [copy_for_each(): lax.all_to_all(jnp.broadcast_to(shard[None], (peers, *shard.shape)), axis...]
  transfers between devices with their start and end apart: 4 -> 11, of which waited for: 4 -> 8; matrix products, arithmetic and copies ran while one was open for 2% -> 9% of each run, Pallas kernels for 0% -> 0%
where the time goes in v1:
time: 327 us
  waiting for transfers between devices  184 us (56%)
  starting transfers between devices  38.9 us (12%)
  blocking collectives  29.1 us (9%)
  local copies, waits for them, and re-layouts  24.5 us (7%)
  matrix products  18.4 us (6%)
  other arithmetic  17.3 us (5%)
  between operations  13.7 us (4%)
    all_gather x1, waiting for transfers between devices, in_one_piece(): whole = lax.all_gather(both, axis, axis=dim, tiled=True)  116 us
    ppermute x7, waiting for transfers between devices, body(): lax.ppermute(ring[-1], 'tp', [(dev, (dev + 1) % 8) for dev in range(8)])  38.6 us
    ppermute x7, starting transfers between devices, body(): lax.ppermute(ring[-1], 'tp', [(dev, (dev + 1) % 8) for dev in range(8)])  22.1 us
    unnamed x40, local copies, waits for them, and re-layouts  20.6 us
    all_to_all x1, blocking collectives, copy_for_each(): lax.all_to_all(jnp.broadcast_to(shard[None], (peers, *shard.shape)), axis...  18.3 us
    all_to_all x1, waiting for transfers between devices, sum_at_owner(): lax.all_to_all(blocks, axis, split_axis=0, concat_axis=0, tiled=True)  15 us
    all_gather x1, waiting for transfers between devices, gathered_once(): both, at, found = (lax.all_gather(jnp.concatenate(lines), axis), 0, {})  14.9 us
    all_to_all x1, starting transfers between devices, sum_at_owner(): lax.all_to_all(blocks, axis, split_axis=0, concat_axis=0, tiled=True)  12.7 us
  transfers between devices with their start and end apart: 11, of which 8 were waited for; matrix products, arithmetic and copies ran while one was open for 9% of the time, Pallas kernels for 0%

profile of v1, /device:TPU:1, one launch (start us, length us, event | category | flops | bytes accessed | tf_op | source)
XLA Modules:
  0.0 326.5 jit_solution(3775686925104905795)
XLA Ops:
  6.5 0.7 negate_log-plus-one_fusion
  7.2 1.1 exponential-minus-one_negate_fusion
  8.8 1.0 copy.41
  10.0 0.9 convert.1
  10.9 15.5 %while.13 = (s32[]{:T(128)}, f32[1,128,128]{2,1,0:T(8,128)S(1)}, f32[4,1,64,128]{3,2,1,0:T(8,128)}, f32[4,1,64,128]{3,2,1,0:T(8,128)S(1)}, f32[4,1,64,128]{3,2,1...) while((s32[]{:T(128)}, f32[1,128,128]{2,1,0:T(8,128)S(1)}, ...), condition=%wide.region_2.3_spmd.clone, body=%wide.region_0.2_spmd.clone.sunk | while | flops 34693120 | bytes 5108864 | solution.py:153
  11.0 0.6 select_exponential_fusion.2
  11.7 1.7 fusion.179
  13.6 0.9 fusion.180
  14.9 0.6 select_exponential_fusion.2
  15.5 1.7 fusion.179
  17.4 0.9 fusion.180
  18.3 0.3 fusion.177
  18.8 0.6 select_exponential_fusion.2
  19.4 1.7 fusion.179
  21.3 0.9 fusion.180
  22.6 0.6 select_exponential_fusion.2
  23.3 1.7 fusion.179
  25.2 0.9 fusion.180
  26.4 10.7 %all-gather.2 = f32[4,129,128]{2,1,0:T(8,128)S(1)} all-gather(f32[1,129,128]{2,1,0:T(8,128)S(1)} %maximum_bitcast_fusion), channel_id=2, replica_groups=mesh['sp_0'=16,'sp_1'=4,'tp'=8] {'sp_1'}, dimensions={0}, use_global_device_ids=true | all-gather | bytes 330240 | tf_op jit(solution)/shard_map/all_gather | solution.py:28
  37.1 0.5 broadcast_select_fusion.3
  37.8 0.6 maximum_bitcast_fusion.1
  38.5 0.7 pad_maximum_fusion
  39.2 4.7 %collective-permute-start = (bf16[128,2048]{1,0:T(8,128)(2,1)S(1)}, bf16[128,2048]{1,0:T(8,128)(2,1)S(1)}, u32[]{:S(2)}, u32[]{:S(2)}) collective-permute-start(bf16[128,2048]{1,0:T(8,128)(2,1)S(1)} %copy-done), channel_id=1, source_target_pairs={{0,1},{1,2},{2,3},{3,4},{4,5},{5,6},{6,7},{7,0},{8,9},{9,10},{10,1... | collective-permute-start | bytes 1572872 | tf_op jit(solution)/shard_map/ppermute | solution.py:189
  43.9 6.1 %collective-permute-done = bf16[128,2048]{1,0:T(8,128)(2,1)S(1)} collective-permute-done((bf16[128,2048]{1,0:T(8,128)(2,1)S(1)}, bf16[128,2048]{1,0:T(8,128)(2,1)S(1)}, u32[]{:S(2)}, u32[]{:S(2)}) %collective-permute-start) | collective-permute-done | bytes 524320 | tf_op jit(solution)/shard_map/ppermute | solution.py:189
  50.0 2.5 collective-permute-start.1
  52.5 6.3 %collective-permute-done.1 = bf16[128,2048]{1,0:T(8,128)(2,1)S(1)} collective-permute-done((bf16[128,2048]{1,0:T(8,128)(2,1)S(1)}, bf16[128,2048]{1,0:T(8,128)(2,1)S(1)}, u32[]{:S(2)}, u32[]{:S(2)}) %collective-permute-start.1) | collective-permute-done | bytes 524320 | tf_op jit(solution)/shard_map/ppermute | solution.py:189
  58.8 2.3 collective-permute-start.2
  61.1 7.6 %collective-permute-done.2 = bf16[128,2048]{1,0:T(8,128)(2,1)S(1)} collective-permute-done((bf16[128,2048]{1,0:T(8,128)(2,1)S(1)}, bf16[128,2048]{1,0:T(8,128)(2,1)S(1)}, u32[]{:S(2)}, u32[]{:S(2)}) %collective-permute-start.2) | collective-permute-done | bytes 524320 | tf_op jit(solution)/shard_map/ppermute | solution.py:189
  68.6 1.1 collective-permute-start.3
  69.7 8.8 %collective-permute-done.3 = bf16[128,2048]{1,0:T(8,128)(2,1)S(1)} collective-permute-done((bf16[128,2048]{1,0:T(8,128)(2,1)S(1)}, bf16[128,2048]{1,0:T(8,128)(2,1)S(1)}, u32[]{:S(2)}, u32[]{:S(2)}) %collective-permute-start.3) | collective-permute-done | bytes 524320 | tf_op jit(solution)/shard_map/ppermute | solution.py:189
  78.5 9.8 %collective-permute-done.4 = bf16[128,2048]{1,0:T(8,128)(2,1)S(1)} collective-permute-done((bf16[128,2048]{1,0:T(8,128)(2,1)S(1)}, bf16[128,2048]{1,0:T(8,128)(2,1)S(1)}, u32[]{:S(2)}, u32[]{:S(2)}) %collective-permute-start.4) | collective-permute-done | bytes 524320 | tf_op jit(solution)/shard_map/ppermute | solution.py:189
  88.3 1.6 copy.47
  89.9 1.6 copy.48
  91.5 14.9 %all-gather.9.cloned.1.call-done = f32[16,129,128]{2,1,0:T(8,128)} async-done(((f32[1,129,128]{2,1,0:T(8,128)}), f32[16,129,128]{2,1,0:T(8,128)}) %all-gather.9.cloned.1.call-update) | async-done | bytes 1056784 | tf_op jit(solution)/shard_map/all_gather | solution.py:28
  106.4 0.8 slice_bitcast_fusion.16
  107.2 11.6 %collective-permute-start.6 = (bf16[128,2048]{1,0:T(8,128)(2,1)}, bf16[128,2048]{1,0:T(8,128)(2,1)}, u32[]{:S(2)}, u32[]{:S(2)}) collective-permute-start(bf16[128,2048]{1,0:T(8,128)(2,1)} %collective-permute-done.5), channel_id=1, source_target_pairs={{0,1},{1,2},{2,3},{3,4},{4,5},{5,6},{6,7},{7,0},{8,9},{9,10},{10,1... | collective-permute-start | bytes 1572872 | tf_op jit(solution)/shard_map/ppermute | solution.py:189
  118.8 2.2 multiply_reduce_fusion.1
  121.0 0.9 fusion.72
  121.9 0.8 broadcast_in_dim.32
  122.7 4.1 %all-to-all-start = ((bf16[8,256,128]{1,2,0:T(8,128)(2,1)}), bf16[8,256,128]{1,2,0:T(8,128)(2,1)}, u32[]{:S(2)}, u32[]{:S(2)}) async-start(bf16[8,256,128]{1,2,0:T(8,128)(2,1)} %broadcast_in_dim.32), calls=%async_computation | async-start | bytes 1048576 | tf_op jit(solution)/shard_map/all_to_all | solution.py:60
  126.9 1.9 constant_dynamic-update-slice_fusion.15
  128.8 1.9 constant_dynamic-update-slice_fusion.14
  130.7 0.8 constant_dynamic-update-slice_fusion.13
  131.6 0.9 constant_dynamic-update-slice_fusion.12
  132.4 0.8 constant_dynamic-update-slice_fusion.11
  133.3 0.8 constant_dynamic-update-slice_fusion.10
  134.1 0.8 constant_dynamic-update-slice_fusion.9
  135.0 0.8 constant_dynamic-update-slice_fusion.8
  135.8 1.9 constant_dynamic-update-slice_fusion.7
  137.7 1.9 constant_dynamic-update-slice_fusion.6
  139.6 0.9 constant_dynamic-update-slice_fusion.5
  140.5 0.8 constant_dynamic-update-slice_fusion.4
  141.3 0.8 constant_dynamic-update-slice_fusion.3
  142.2 0.9 constant_dynamic-update-slice_fusion.2
  143.0 0.9 constant_dynamic-update-slice_fusion.1
  143.9 0.9 constant_dynamic-update-slice_fusion
  144.8 4.0 %multiply_reduce_fusion = (f32[256]{0:T(256)S(1)}, f32[256,2048]{1,0:T(8,128)S(1)}) fusion(bf16[256,1024]{0,1:T(8,128)(2,1)} %bitcast.42, bf16[2048,2048]{1,0:T(8,128)(2,1)} %constant_dynamic-update-slice_fusion, s32[]{:T(128)S(6)} %select_n.294, bf16[256,2048]{1,0:T(8,128)(2,1)} %param.14), kind=kOutput, calls=%fused_computation.47 | convolution fusion | flops 1075838720 | bytes 7865348 | tf_op jit(solution)/shard_map/dot_general | solution.py:193
  148.8 115.8 %all-gather.7.cloned.1.call-done = bf16[2048,2048]{1,0:T(8,128)(2,1)} async-done(((bf16[32,2048]{1,0:T(8,128)(2,1)}), bf16[2048,2048]{1,0:T(8,128)(2,1)}) %all-gather.7.cloned.1.call-update) | async-done | bytes 8388624 | tf_op jit(solution)/shard_map/all_gather | solution.py:72
  264.7 6.8 %fusion.37 = bf16[256,2048]{1,0:T(8,128)(2,1)} fusion(bf16[2048,2048]{1,0:T(8,128)(2,1)} %all-gather.7.cloned.1.call-done, f32[256,2048]{1,0:T(8,128)S(1)} %get-tuple-element.142, f32[2048]{0:T(1024)S(1)} %copy-done.9, f32[256]{0:T(256)S(1)} %add_rsqrt_fusion), kind=kOutput, calls=%fused_computation.44 | convolution fusion | flops 2150367232 | bytes 11543552 | tf_op jit(solution)/shard_map/dot_general | solution.py:205
  271.5 12.7 %all-to-all-start.1 = ((bf16[8,32,2048]{2,1,0:T(8,128)(2,1)}), bf16[8,32,2048]{2,1,0:T(8,128)(2,1)S(1)}, u32[]{:S(2)}, u32[]{:S(2)}) async-start(bf16[8,32,2048]{2,1,0:T(8,128)(2,1)} %bitcast.43), calls=%async_computation.1 | async-start | bytes 2097152 | tf_op jit(solution)/shard_map/all_to_all | solution.py:84
  284.2 15.0 %all-to-all-done.1 = bf16[8,32,2048]{2,1,0:T(8,128)(2,1)S(1)} async-done(((bf16[8,32,2048]{2,1,0:T(8,128)(2,1)}), bf16[8,32,2048]{2,1,0:T(8,128)(2,1)S(1)}, u32[]{:S(2)}, u32[]{:S(2)}) %all-to-all-start.1) | async-done | bytes 1048608 | tf_op jit(solution)/shard_map/all_to_all | solution.py:84
  299.3 1.0 add_convert_fusion
  300.4 18.3 %all_to_all.15 = bf16[8,32,2048]{2,1,0:T(8,128)(2,1)S(1)} all-to-all(bf16[8,32,2048]{2,1,0:T(8,128)(2,1)S(1)} %broadcast_in_dim.33), channel_id=1, replica_groups=mesh['sp_0'=16,'sp_1'=4,'tp'=8] {'tp'}, dimensions={0} | all-to-all | bytes 2097152 | tf_op jit(solution)/shard_map/all_to_all | solution.py:60
  318.7 1.0 copy.95
  (82 shorter events, 3.4 us)
Async XLA Ops:
  6.5 99.8 %all-gather.9.cloned.1.call-start = ((), (), s32[]{:S(2)}) async-start(), calls=%async_computation.4 | async-start | bytes 1183744 | tf_op jit(solution)/shard_map/all_gather | solution.py:28
  9.8 1.0 copy-start.1
  10.9 27.6 %copy-start.2 = (bf16[32,1024]{1,0:T(8,128)(2,1)S(1)}, bf16[32,1024]{1,0:T(8,128)(2,1)}, u32[]{:S(2)}) copy-start(bf16[32,1024]{1,0:T(8,128)(2,1)} %param.25) | copy-start | bytes 196612
  10.9 27.6 %copy-start.3 = (bf16[32,1024]{1,0:T(8,128)(2,1)S(1)}, bf16[32,1024]{1,0:T(8,128)(2,1)}, u32[]{:S(2)}) copy-start(bf16[32,1024]{1,0:T(8,128)(2,1)} %param.24) | copy-start | bytes 196612
  10.9 28.3 %copy-start = (bf16[128,2048]{1,0:T(8,128)(2,1)S(1)}, bf16[128,2048]{1,0:T(8,128)(2,1)}, u32[]{:S(2)}) copy-start(bf16[128,2048]{1,0:T(8,128)(2,1)} %param.22) | copy-start | bytes 1572868
  37.1 2.0 copy-start.6
  37.1 2.0 copy-start.7
  37.1 2.0 copy-start.8
  37.6 1.5 copy-start.5
  38.4 226.2 %all-gather.7.cloned.1.call-start = ((), (), s32[]{:S(2)}) async-start(), calls=%async_computation.3 | async-start | bytes 8519680 | tf_op jit(solution)/shard_map/all_gather | solution.py:72
  39.2 10.8 %collective-permute-start = (bf16[128,2048]{1,0:T(8,128)(2,1)S(1)}, bf16[128,2048]{1,0:T(8,128)(2,1)S(1)}, u32[]{:S(2)}, u32[]{:S(2)}) collective-permute-start(bf16[128,2048]{1,0:T(8,128)(2,1)S(1)} %copy-done), channel_id=1, source_target_pairs={{0,1},{1,2},{2,3},{3,4},{4,5},{5,6},{6,7},{7,0},{8,9},{9,10},{10,1... | collective-permute-start | bytes 1572872 | tf_op jit(solution)/shard_map/ppermute | solution.py:189
  50.0 8.8 %collective-permute-start.1 = (bf16[128,2048]{1,0:T(8,128)(2,1)S(1)}, bf16[128,2048]{1,0:T(8,128)(2,1)S(1)}, u32[]{:S(2)}, u32[]{:S(2)}) collective-permute-start(bf16[128,2048]{1,0:T(8,128)(2,1)S(1)} %collective-permute-done), channel_id=1, source_target_pairs={{0,1},{1,2},{2,3},{3,4},{4,5},{5,6},{6,7},{7,0},{8,9},{9,10},{10,1... | collective-permute-start | bytes 1572872 | tf_op jit(solution)/shard_map/ppermute | solution.py:189
  58.8 9.8 %collective-permute-start.2 = (bf16[128,2048]{1,0:T(8,128)(2,1)S(1)}, bf16[128,2048]{1,0:T(8,128)(2,1)S(1)}, u32[]{:S(2)}, u32[]{:S(2)}) collective-permute-start(bf16[128,2048]{1,0:T(8,128)(2,1)S(1)} %collective-permute-done.1), channel_id=1, source_target_pairs={{0,1},{1,2},{2,3},{3,4},{4,5},{5,6},{6,7},{7,0},{8,9},{9,10},{10,1... | collective-permute-start | bytes 1572872 | tf_op jit(solution)/shard_map/ppermute | solution.py:189
  68.6 9.8 %collective-permute-start.3 = (bf16[128,2048]{1,0:T(8,128)(2,1)S(1)}, bf16[128,2048]{1,0:T(8,128)(2,1)S(1)}, u32[]{:S(2)}, u32[]{:S(2)}) collective-permute-start(bf16[128,2048]{1,0:T(8,128)(2,1)S(1)} %collective-permute-done.2), channel_id=1, source_target_pairs={{0,1},{1,2},{2,3},{3,4},{4,5},{5,6},{6,7},{7,0},{8,9},{9,10},{10,1... | collective-permute-start | bytes 1572872 | tf_op jit(solution)/shard_map/ppermute | solution.py:189
  78.5 9.8 %collective-permute-start.4 = (bf16[128,2048]{1,0:T(8,128)(2,1)S(1)}, bf16[128,2048]{1,0:T(8,128)(2,1)S(1)}, u32[]{:S(2)}, u32[]{:S(2)}) collective-permute-start(bf16[128,2048]{1,0:T(8,128)(2,1)S(1)} %collective-permute-done.3), channel_id=1, source_target_pairs={{0,1},{1,2},{2,3},{3,4},{4,5},{5,6},{6,7},{7,0},{8,9},{9,10},{10,1... | collective-permute-start | bytes 1572872 | tf_op jit(solution)/shard_map/ppermute | solution.py:189
  88.3 18.9 %collective-permute-start.5 = (bf16[128,2048]{1,0:T(8,128)(2,1)S(1)}, bf16[128,2048]{1,0:T(8,128)(2,1)}, u32[]{:S(2)}, u32[]{:S(2)}) collective-permute-start(bf16[128,2048]{1,0:T(8,128)(2,1)S(1)} %collective-permute-done.4), channel_id=1, source_target_pairs={{0,1},{1,2},{2,3},{3,4},{4,5},{5,6},{6,7},{7,0},{8,9},{9,10},{10,1... | collective-permute-start | bytes 1572872 | tf_op jit(solution)/shard_map/ppermute | solution.py:189
  107.2 19.7 %collective-permute-start.6 = (bf16[128,2048]{1,0:T(8,128)(2,1)}, bf16[128,2048]{1,0:T(8,128)(2,1)}, u32[]{:S(2)}, u32[]{:S(2)}) collective-permute-start(bf16[128,2048]{1,0:T(8,128)(2,1)} %collective-permute-done.5), channel_id=1, source_target_pairs={{0,1},{1,2},{2,3},{3,4},{4,5},{5,6},{6,7},{7,0},{8,9},{9,10},{10,1... | collective-permute-start | bytes 1572872 | tf_op jit(solution)/shard_map/ppermute | solution.py:189
  122.7 22.0 %all-to-all-start = ((bf16[8,256,128]{1,2,0:T(8,128)(2,1)}), bf16[8,256,128]{1,2,0:T(8,128)(2,1)}, u32[]{:S(2)}, u32[]{:S(2)}) async-start(bf16[8,256,128]{1,2,0:T(8,128)(2,1)} %broadcast_in_dim.32), calls=%async_computation | async-start | bytes 1048576 | tf_op jit(solution)/shard_map/all_to_all | solution.py:60
  135.8 128.9 %copy-start.9 = (f32[2048]{0:T(1024)S(1)}, f32[2048]{0:T(1024)}, u32[]{:S(2)}) copy-start(f32[2048]{0:T(1024)} %param.23) | copy-start | bytes 24580
  148.8 122.7 %copy-start.4 = (f32[256,2048]{1,0:T(8,128)}, f32[256,2048]{1,0:T(8,128)S(1)}, u32[]{:S(2)}) copy-start(f32[256,2048]{1,0:T(8,128)S(1)} %get-tuple-element.142) | copy-start | bytes 6291460
  271.5 27.6 %all-to-all-start.1 = ((bf16[8,32,2048]{2,1,0:T(8,128)(2,1)}), bf16[8,32,2048]{2,1,0:T(8,128)(2,1)S(1)}, u32[]{:S(2)}, u32[]{:S(2)}) async-start(bf16[8,32,2048]{2,1,0:T(8,128)(2,1)} %bitcast.43), calls=%async_computation.1 | async-start | bytes 2097152 | tf_op jit(solution)/shard_map/all_to_all | solution.py:84
Sparse Core Ops, SparseCore 0:
  38.6 67.7 all-gather.8
  109.3 155.2 all-gather.6
